TPU v7x, 32 devices: a whole 2x2x4 slice. The times are simulated.
32 devices in a mesh: grp: 2 (over x), ep: 16 (over z, y, core).
Axes of the slice: x: 2, y: 2, z: 4, core: 2. Of those that a mesh axis runs over, the one named last changes fastest.
Arguments:
- hidden: bfloat16 [224, 2048], P(('grp', 'ep')), parts along dimension 0, may hold values from -6 to 6
- state_in: float32 [224, 64, 4096], P(('grp', 'ep')), parts along dimension 0, may hold values from -4 to 4
- conv_state: bfloat16 [224, 3, 4608], P(('grp', 'ep')), parts along dimension 0, may hold values from -6 to 6
- expert_ids: int32 [224, 4], P(('grp', 'ep')), parts along dimension 0, may hold values from 0 to 15, as said below
- group_prob: float32 [224], P(('grp', 'ep')), parts along dimension 0, may hold values from 0.25 to 1
- expert_score: float32 [224, 4], P(('grp', 'ep')), parts along dimension 0, may hold values from 0.05 to 1
- first_gain: bfloat16 [2048], replicated, may hold values from 0.099609375 to 1.8984375
- z_weight: bfloat16 [2048, 4096], P(None, 'ep'), may hold values from -0.125 to 0.125
- x_weight: bfloat16 [2048, 4096], P(None, 'ep'), may hold values from -0.125 to 0.125
- b_weight: bfloat16 [2048, 256], replicated, may hold values from -0.125 to 0.125
- c_weight: bfloat16 [2048, 256], replicated, may hold values from -0.125 to 0.125
- dt_weight: bfloat16 [2048, 64], replicated, may hold values from -0.125 to 0.125
- conv_weight: bfloat16 [4, 4608], replicated, may hold values from -3 to 3
- conv_bias: bfloat16 [4608], replicated, may hold values from -3 to 3
- dt_bias: float32 [64], replicated, may hold values from -4 to 0
- decay_log: float32 [64], replicated, may hold values from 0 to 2
- skip_gain: float32 [64], replicated, may hold values from 0.1 to 1.9
- inner_gain: bfloat16 [4096], replicated, may hold values from 0.099609375 to 1.8984375
- out_weight: bfloat16 [4096, 2048], P(None, 'ep'), may hold values from -0.09375 to 0.09375
- second_gain: bfloat16 [2048], replicated, may hold values from 0.099609375 to 1.8984375
- expert_gate: bfloat16 [16, 2048, 512], P('ep'), may hold values from -0.125 to 0.125
- expert_up: bfloat16 [16, 2048, 512], P('ep'), may hold values from -0.125 to 0.125
- expert_down: bfloat16 [16, 512, 2048], P('ep'), may hold values from -0.25 to 0.25
Outputs:
- layer_out: bfloat16 [224, 2048], P(('grp', 'ep')), parts along dimension 0
- state_out: float32 [224, 64, 4096], P(('grp', 'ep')), parts along dimension 0
- conv_out: bfloat16 [224, 3, 4608], P(('grp', 'ep')), parts along dimension 0
There are 2 independent parts, one for each index of `grp`. A program takes and returns all parts, laid end to end along the dimension named above; an argument that names none is the same for every part. Nothing has to cross between parts.
Inputs may be any that keep to these rules, and one draw needn't show every extreme that they name: `expert_ids`: each row names 4 different experts of one expert group (numbers g * 8 to g * 8 + 7). Among the 7 rows of one device no expert is named more than 3 times, and in every draw one expert is named exactly 3 times by the rows of every device.
All inputs are finite; a program needn't handle non-finite values.
Results may differ from a plain program's by a relative error of at most 0.014.
Values may be sent and summed in bfloat16 or wider, within the bound.
No kernel may reach another device: no remote copies, remote signals or barrier semaphores. Data moves between devices by JAX's collectives and lax.ppermute only.
A program may use at most 128 MiB of HBM per device.

v0:
```python
import jax
import jax.numpy as jnp
from jax import lax
from jax.sharding import PartitionSpec as P

HEADS = 64
HEAD_DIM = 64
SSM_GROUPS = 4
STATE = 64
TOP = 4
EPS = 1e-06


def rms_scale(values, gain_vec):
    return (
        values
        * lax.rsqrt(jnp.mean(values * values, axis=-1, keepdims=True) + EPS)
        * gain_vec.astype(jnp.float32)
    )


def state_step(active, dt_raw, state_in, dt_bias, decay_log, skip_gain):
    row_count = active.shape[0]
    inner_width = HEADS * HEAD_DIM
    state_span = SSM_GROUPS * STATE
    per_group = HEADS // SSM_GROUPS
    x_heads = active[:, :inner_width].reshape(row_count, HEADS, HEAD_DIM)
    b_input = active[:, inner_width : inner_width + state_span].reshape(
        row_count, SSM_GROUPS, STATE
    )
    c_input = active[:, inner_width + state_span :].reshape(row_count, SSM_GROUPS, STATE)
    b_heads = jnp.repeat(b_input, per_group, axis=1)
    c_heads = jnp.repeat(c_input, per_group, axis=1)
    step_size = jax.nn.softplus(dt_raw.astype(jnp.float32) + dt_bias[None, :])
    decay_rate = jnp.exp(-step_size * jnp.exp(decay_log)[None, :])
    carried = state_in.reshape(row_count, HEADS, HEAD_DIM, STATE)
    carried = (
        decay_rate[:, :, None, None] * carried
        + (step_size[:, :, None] * x_heads)[:, :, :, None] * b_heads[:, :, None, :]
    )
    readout = jnp.einsum("bhpn,bhn->bhp", carried, c_heads, precision=lax.Precision.HIGHEST)
    readout = readout + skip_gain[None, :, None] * x_heads
    return (
        readout.reshape(row_count, inner_width),
        carried.reshape(row_count, HEADS, HEAD_DIM * STATE),
    )


def body(
    hidden,
    state_in,
    conv_state,
    expert_ids,
    group_prob,
    expert_score,
    first_gain,
    z_weight,
    x_weight,
    b_weight,
    c_weight,
    dt_weight,
    conv_weight,
    conv_bias,
    dt_bias,
    decay_log,
    skip_gain,
    inner_gain,
    out_weight,
    second_gain,
    expert_gate,
    expert_up,
    expert_down,
):
    row_count = hidden.shape[0]
    model_width = hidden.shape[1]
    normed = rms_scale(hidden.astype(jnp.float32), first_gain).astype(jnp.bfloat16)
    row_part = lax.all_gather(normed, "ep", axis=0, tiled=True)
    both_parts = jnp.concatenate(
        [
            jnp.dot(row_part, z_weight, preferred_element_type=jnp.float32),
            jnp.dot(row_part, x_weight, preferred_element_type=jnp.float32),
        ],
        axis=1,
    )
    projected_both = both_parts.astype(jnp.bfloat16)
    col_count = z_weight.shape[1]
    gate_z, x_part = (
        lax.all_to_all(
            projected_both[:, :col_count], "ep", split_axis=0, concat_axis=1, tiled=True
        ),
        lax.all_to_all(
            projected_both[:, col_count:], "ep", split_axis=0, concat_axis=1, tiled=True
        ),
    )
    b_part = jnp.dot(normed, b_weight, preferred_element_type=jnp.float32).astype(jnp.bfloat16)
    c_part = jnp.dot(normed, c_weight, preferred_element_type=jnp.float32).astype(jnp.bfloat16)
    dt_raw = jnp.dot(normed, dt_weight, preferred_element_type=jnp.float32).astype(jnp.bfloat16)
    fresh_input = jnp.concatenate([x_part, b_part, c_part], axis=1)
    window = jnp.concatenate([conv_state, fresh_input[:, None, :]], axis=1)
    summed = jnp.sum(window.astype(jnp.float32) * conv_weight.astype(jnp.float32)[None], axis=1)
    active = jax.nn.silu(summed + conv_bias.astype(jnp.float32)[None, :])
    readout, state_out = state_step(active, dt_raw, state_in, dt_bias, decay_log, skip_gain)
    gated = readout * jax.nn.silu(gate_z.astype(jnp.float32))
    y_mix = rms_scale(gated, inner_gain).astype(jnp.bfloat16)
    slice_out = jnp.dot(
        lax.all_gather(y_mix, "ep", axis=0, tiled=True),
        out_weight,
        preferred_element_type=jnp.float32,
    ).astype(jnp.bfloat16)
    projected = lax.all_to_all(slice_out, "ep", split_axis=0, concat_axis=1, tiled=True)
    projected = lax.optimization_barrier(projected)
    mixed_rows = (hidden.astype(jnp.float32) + projected.astype(jnp.float32)).astype(jnp.bfloat16)
    normed2 = rms_scale(mixed_rows.astype(jnp.float32), second_gain).astype(jnp.bfloat16)
    expert_count = lax.axis_size("ep")
    capacity = max(2, (3 * row_count * TOP + 2 * expert_count - 1) // (2 * expert_count))
    slot_total = expert_count * capacity
    flat_ids = expert_ids.reshape(-1)
    one_hot = (flat_ids[:, None] == jnp.arange(expert_count, dtype=jnp.int32)[None, :]).astype(
        jnp.int32
    )
    earlier = jnp.cumsum(one_hot, axis=0) - one_hot
    slot_rank = jnp.sum(earlier * one_hot, axis=1)
    slot_place = (flat_ids * capacity + slot_rank).reshape(row_count, TOP)
    slot_index = jnp.arange(slot_total, dtype=jnp.int32)
    dispatch = jnp.sum(
        (slot_index[:, None, None] == slot_place[None, :, :]).astype(jnp.int32), axis=2
    )
    outgoing = jnp.dot(dispatch.astype(jnp.bfloat16), normed2, preferred_element_type=jnp.float32)
    outgoing = outgoing.astype(jnp.bfloat16).reshape(expert_count, capacity, model_width)
    arrived = lax.all_to_all(outgoing, "ep", split_axis=0, concat_axis=0, tiled=True)
    sources, slots_here, width = arrived.shape
    flattened = arrived.reshape(sources * slots_here, width)
    gate_part = jnp.dot(flattened, expert_gate[0], preferred_element_type=jnp.float32)
    up_part = jnp.dot(flattened, expert_up[0], preferred_element_type=jnp.float32)
    hidden_act = (jax.nn.silu(gate_part) * up_part).astype(jnp.bfloat16)
    expert_out = jnp.dot(hidden_act, expert_down[0], preferred_element_type=jnp.float32).astype(
        jnp.bfloat16
    )
    returned = lax.all_to_all(
        expert_out.reshape(sources, slots_here, width),
        "ep",
        split_axis=0,
        concat_axis=0,
        tiled=True,
    )
    returned = returned.reshape(slot_total, model_width)
    route_share = group_prob[:, None] * expert_score / jnp.sum(expert_score, axis=1, keepdims=True)
    moe_sum = jnp.zeros((row_count, model_width), jnp.float32)
    for pick in range(TOP):
        select_rows = (slot_place[:, pick][:, None] == slot_index[None, :]).astype(jnp.bfloat16)
        picked = jnp.dot(select_rows, returned, preferred_element_type=jnp.float32)
        moe_sum = moe_sum + route_share[:, pick : pick + 1] * picked
    layer_out = (mixed_rows.astype(jnp.float32) + moe_sum).astype(jnp.bfloat16)
    return (layer_out, state_out, window[:, 1:, :])


def solution(mesh):
    in_specs = (
        P(("grp", "ep"), None),
        P(("grp", "ep"), None, None),
        P(("grp", "ep"), None, None),
        P(("grp", "ep"), None),
        P(("grp", "ep")),
        P(("grp", "ep"), None),
        P(),
        P(None, "ep"),
        P(None, "ep"),
        P(),
        P(),
        P(),
        P(),
        P(),
        P(),
        P(),
        P(),
        P(),
        P(None, "ep"),
        P(),
        P("ep", None, None),
        P("ep", None, None),
        P("ep", None, None),
    )
    out_specs = (P(("grp", "ep"), None), P(("grp", "ep"), None, None), P(("grp", "ep"), None, None))
    return jax.shard_map(body, mesh=mesh, in_specs=in_specs, out_specs=out_specs, check_vma=False)
```

profile of v0, /device:TPU:0, one launch (start us, length us, event | category | flops | bytes accessed | tf_op | source)
XLA Modules:
  0.0 186.1 jit_solution(1612493214570379041)
XLA Ops:
  0.6 0.8 convert_element_type.99
  1.5 0.9 fusion.30
  2.4 0.8 fusion.52
  3.2 24.6 %all-gather = bf16[16,7,2048]{2,1,0:T(8,128)(2,1)S(1)} all-gather(bf16[1,7,2048]{2,1,0:T(8,128)(2,1)S(1)} %fusion.52), channel_id=1, replica_groups=mesh['grp'=2,'ep'=16] {'ep'}, dimensions={0}, use_global_device_ids=true | all-gather | bytes 487424 | tf_op jit(solution)/shard_map/all_gather | solution.py:77
  27.8 0.2 reshape.119
  28.0 1.5 convolution_convert_fusion.3
  29.5 0.7 all_to_all.44
  30.2 3.5 %all-to-all-start = ((bf16[16,7,256]{2,1,0:T(8,128)(2,1)}), bf16[16,7,256]{2,1,0:T(8,128)(2,1)S(1)}, u32[]{:S(2)}, u32[]{:S(2)}) async-start(bf16[16,7,256]{2,1,0:T(8,128)(2,1)} %all_to_all.44), calls=%async_computation | async-start | bytes 131072 | tf_op jit(solution)/shard_map/all_to_all | solution.py:91
  33.7 1.5 convolution_convert_fusion.5
  35.2 1.5 convolution_convert_fusion.6
  36.7 0.8 convert_element_type.106
  37.5 0.7 convert_element_type.107
  38.2 0.7 exp.26
  39.0 12.7 %reshape.106 = f32[7,64,64,64]{3,2,1,0:T(8,128)} reshape(f32[7,64,4096]{2,1,0:T(8,128)} %param.24) | data formatting | bytes 14680064 | tf_op jit(solution)/shard_map/reshape | solution.py:36
  51.7 1.5 convolution_convert_fusion.2
  53.3 0.7 all_to_all.48
  54.2 0.2 select_reduce_fusion
  54.7 0.2 multiply_exponential_fusion
  55.0 0.2 slice_reduce_fusion
  55.2 6.0 %all-to-all-start.1 = ((bf16[16,7,256]{2,1,0:T(8,128)(2,1)}), bf16[16,7,256]{2,1,0:T(8,128)(2,1)S(1)}, u32[]{:S(2)}, u32[]{:S(2)}) async-start(bf16[16,7,256]{2,1,0:T(8,128)(2,1)} %all_to_all.48), calls=%async_computation.1 | async-start | bytes 131072 | tf_op jit(solution)/shard_map/all_to_all | solution.py:88
  61.7 6.4 %all-to-all-done.1 = bf16[16,7,256]{2,1,0:T(8,128)(2,1)S(1)} async-done(((bf16[16,7,256]{2,1,0:T(8,128)(2,1)}), bf16[16,7,256]{2,1,0:T(8,128)(2,1)S(1)}, u32[]{:S(2)}, u32[]{:S(2)}) %all-to-all-start.1) | async-done | bytes 57376 | tf_op jit(solution)/shard_map/all_to_all | solution.py:88
  68.3 0.1 broadcast_multiply_fusion.2
  68.5 26.7 %fusion = f32[7,64,1,64]{3,2,1,0:T(1,128)S(1)} fusion(f32[7,64,64,1]{2,3,1,0:T(1,128)S(1)} %bitcast.68, f32[7,64,64,64]{3,2,1,0:T(8,128)} %reshape.106, f32[7,64]{1,0:T(8,128)S(1)} %get-tuple-element.17, f32[7,64,64]{2,1,0:T(8,128)S(1)} %bitcast.65, f32[7,64,64]{2,1,0:T(8,128)S(1)} %broadcast_multiply_fusion.2), kind=kOutput, calls=%fused_computation | convolution fusion | flops 27525120 | bytes 7800576 | tf_op jit(solution)/shard_map/bhpn,bhn->bhp/dot_general | solution.py:41
  95.1 0.2 multiply_reduce_fusion.1
  95.6 20.7 %all-gather.1 = bf16[16,7,4096]{2,1,0:T(8,128)(2,1)S(1)} all-gather(bf16[1,7,4096]{2,1,0:T(8,128)(2,1)S(1)} %fusion.37), channel_id=1, replica_groups=mesh['grp'=2,'ep'=16] {'ep'}, dimensions={0}, use_global_device_ids=true | all-gather | bytes 974848 | tf_op jit(solution)/shard_map/all_gather | solution.py:106
  116.3 1.2 reshape.121
  117.6 1.9 %convolution_convert_fusion.4 = bf16[112,128]{1,0:T(8,128)(2,1)S(1)} fusion(bf16[112,4096]{1,0:T(8,128)(2,1)} %reshape.121, bf16[4096,128]{1,0:T(8,128)(2,1)} %param.41), kind=kOutput, calls=%fused_computation.26 | convolution fusion | flops 117454848 | bytes 1994752 | tf_op jit(solution)/shard_map/dot_general | solution.py:105
  119.5 0.6 all_to_all.50
  120.1 3.5 %all-to-all-start.2 = ((bf16[16,7,128]{2,1,0:T(8,128)(2,1)}), bf16[16,7,128]{2,1,0:T(8,128)(2,1)S(1)}, u32[]{:S(2)}, u32[]{:S(2)}) async-start(bf16[16,7,128]{2,1,0:T(8,128)(2,1)} %all_to_all.50), calls=%async_computation.2 | async-start | bytes 65536 | tf_op jit(solution)/shard_map/all_to_all | solution.py:110
  123.6 8.7 %broadcast_multiply_fusion = f32[7,64,64,64]{3,2,1,0:T(8,128)} fusion(f32[7,64,64]{2,1,0:T(8,128)} %bitcast.66, f32[7,64,64]{2,1,0:T(8,128)S(1)} %broadcast_multiply_fusion.2), kind=kLoop, calls=%fused_computation.4 | loop fusion | flops 1835008 | bytes 7569408 | tf_op jit(solution)/shard_map/mul | solution.py:39
  132.3 12.9 %mul.261 = f32[7,64,4096]{2,1,0:T(8,128)} reshape(f32[7,64,64,64]{3,2,1,0:T(8,128)} %broadcast_multiply_fusion) | data formatting | bytes 14680064 | tf_op jit(solution)/shard_map/mul | solution.py:39
  145.1 0.1 fusion.34
  145.3 0.3 convolution_convert_fusion.1
  145.6 0.8 reshape.112
  146.4 6.0 %all-to-all-start.3 = ((bf16[16,3,2048]{2,1,0:T(4,128)(2,1)}), bf16[16,3,2048]{2,1,0:T(4,128)(2,1)S(1)}, u32[]{:S(2)}, u32[]{:S(2)}) async-start(bf16[16,3,2048]{2,1,0:T(4,128)(2,1)} %reshape.112), calls=%async_computation.3 | async-start | bytes 524288 | tf_op jit(solution)/shard_map/all_to_all | solution.py:130
  152.4 10.6 %multiply_add_fusion = f32[7,64,4096]{2,1,0:T(8,128)} fusion(f32[7,64,4096]{2,1,0:T(8,128)} %mul.261, f32[7,64,4096]{2,1,0:T(8,128)} %param.24, f32[7,64]{1,0:T(8,128)S(1)} %get-tuple-element.17), kind=kLoop, calls=%fused_computation.3 | loop fusion | flops 3670016 | bytes 22021888 | tf_op jit(solution)/shard_map/add | solution.py:38
  162.9 0.2 reshape.113
  163.1 2.0 %fusion.12 = f32[48,512]{1,0:T(8,128)S(1)} fusion(bf16[48,2048]{1,0:T(8,128)(2,1)S(1)} %reshape.113, bf16[1,2048,512]{2,1,0:T(8,128)(2,1)} %param.43), kind=kOutput, calls=%fused_computation.20 | convolution fusion | flops 100663296 | bytes 2392064 | tf_op jit(solution)/shard_map/dot_general | solution.py:133
  165.2 2.5 %convolution_convert_fusion = bf16[48,2048]{1,0:T(8,128)(2,1)S(1)} fusion(bf16[1,512,2048]{2,1,0:T(8,128)(2,1)S(1)} %copy-done, bf16[48,2048]{1,0:T(8,128)(2,1)S(1)} %reshape.113, bf16[1,2048,512]{2,1,0:T(8,128)(2,1)} %param.44, f32[48,512]{1,0:T(8,128)S(1)} %fusion.12), kind=kOutput, calls=%fused_computation.6 | convolution fusion | flops 201572352 | bytes 4685824 | tf_op jit(solution)/shard_map/dot_general | solution.py:136
  167.7 0.8 reshape.114
  168.5 6.0 %all-to-all-start.4 = ((bf16[16,3,2048]{2,1,0:T(4,128)(2,1)}), bf16[16,3,2048]{2,1,0:T(4,128)(2,1)S(1)}, u32[]{:S(2)}, u32[]{:S(2)}) async-start(bf16[16,3,2048]{2,1,0:T(4,128)(2,1)} %reshape.114), calls=%async_computation.4 | async-start | bytes 524288 | tf_op jit(solution)/shard_map/all_to_all | solution.py:139
  174.5 0.7 fusion.24
  175.3 9.3 %all-to-all-done.4 = bf16[16,3,2048]{2,1,0:T(4,128)(2,1)S(1)} async-done(((bf16[16,3,2048]{2,1,0:T(4,128)(2,1)}), bf16[16,3,2048]{2,1,0:T(4,128)(2,1)S(1)}, u32[]{:S(2)}, u32[]{:S(2)}) %all-to-all-start.4) | async-done | bytes 196640 | tf_op jit(solution)/shard_map/all_to_all | solution.py:139
  184.5 0.2 reshape.115
  184.7 0.2 convolution_multiply_fusion.3
  184.9 0.2 fusion.7
  185.1 0.2 fusion.6
  185.3 0.8 fusion.8
  (59 shorter events, 1.5 us)
Async XLA Ops:
  0.6 164.5 %copy-start = (bf16[1,512,2048]{2,1,0:T(8,128)(2,1)S(1)}, bf16[1,512,2048]{2,1,0:T(8,128)(2,1)}, u32[]{:S(2)}) copy-start(bf16[1,512,2048]{2,1,0:T(8,128)(2,1)} %param.45) | copy-start | bytes 6291460
  30.2 25.0 %all-to-all-start = ((bf16[16,7,256]{2,1,0:T(8,128)(2,1)}), bf16[16,7,256]{2,1,0:T(8,128)(2,1)S(1)}, u32[]{:S(2)}, u32[]{:S(2)}) async-start(bf16[16,7,256]{2,1,0:T(8,128)(2,1)} %all_to_all.44), calls=%async_computation | async-start | bytes 131072 | tf_op jit(solution)/shard_map/all_to_all | solution.py:91
  38.9 15.0 %copy-start.5 = (bf16[4096]{0:T(1024)(128)(2,1)S(1)}, bf16[4096]{0:T(1024)(128)(2,1)}, u32[]{:S(2)}) copy-start(bf16[4096]{0:T(1024)(128)(2,1)} %param.40) | copy-start | bytes 24580
  38.9 15.0 %copy-start.8 = (s32[7,4]{0,1:T(4,128)S(1)}, s32[7,4]{0,1:T(4,128)}, u32[]{:S(2)}) copy-start(s32[7,4]{0,1:T(4,128)} %param.26) | copy-start | bytes 340
  38.9 15.7 %copy-start.7 = (bf16[2048]{0:T(1024)(128)(2,1)S(1)}, bf16[2048]{0:T(1024)(128)(2,1)}, u32[]{:S(2)}) copy-start(bf16[2048]{0:T(1024)(128)(2,1)} %param.42) | copy-start | bytes 12292
  38.9 15.7 %copy-start.6 = (f32[7,4]{0,1:T(4,128)S(1)}, f32[7,4]{0,1:T(4,128)}, u32[]{:S(2)}) copy-start(f32[7,4]{0,1:T(4,128)} %param.28) | copy-start | bytes 340
  38.9 15.7 %copy-start.10 = (f32[7]{0:T(128)S(1)}, f32[7]{0:T(128)}, u32[]{:S(2)}) copy-start(f32[7]{0:T(128)} %param.27) | copy-start | bytes 88
  38.9 15.8 %copy-start.2 = (bf16[7,2048]{1,0:T(8,128)(2,1)S(1)}, bf16[7,2048]{1,0:T(8,128)(2,1)}, u32[]{:S(2)}) copy-start(bf16[7,2048]{1,0:T(8,128)(2,1)} %param.23) | copy-start | bytes 86020
  38.9 15.8 %copy-start.11 = (bf16[2048,64]{0,1:T(8,128)(2,1)S(1)}, bf16[2048,64]{0,1:T(8,128)(2,1)}, u32[]{:S(2)}) copy-start(bf16[2048,64]{0,1:T(8,128)(2,1)} %param.34) | copy-start | bytes 786436
  39.0 15.8 %copy-start.12 = (f32[64]{0:T(128)S(1)}, f32[64]{0:T(128)}, u32[]{:S(2)}) copy-start(f32[64]{0:T(128)} %param.37) | copy-start | bytes 772
  39.0 22.3 %copy-start.3 = (bf16[7,3,4608]{2,0,1:T(8,128)(2,1)S(1)}, bf16[7,3,4608]{2,0,1:T(8,128)(2,1)}, u32[]{:S(2)}) copy-start(bf16[7,3,4608]{2,0,1:T(8,128)(2,1)} %param.25) | copy-start | bytes 580612
  55.2 12.9 %all-to-all-start.1 = ((bf16[16,7,256]{2,1,0:T(8,128)(2,1)}), bf16[16,7,256]{2,1,0:T(8,128)(2,1)S(1)}, u32[]{:S(2)}, u32[]{:S(2)}) async-start(bf16[16,7,256]{2,1,0:T(8,128)(2,1)} %all_to_all.48), calls=%async_computation.1 | async-start | bytes 131072 | tf_op jit(solution)/shard_map/all_to_all | solution.py:88
  68.4 26.7 %copy-start.1 = (f32[7,4,16,64]{3,2,1,0:T(8,128)}, f32[7,4,16,64]{3,2,1,0:T(8,128)S(1)}, u32[]{:S(2)}) copy-start(f32[7,4,16,64]{3,2,1,0:T(8,128)S(1)} %broadcast_in_dim.7) | copy-start | bytes 344068
  68.5 26.7 %copy-start.9 = (f32[64]{0:T(128)S(1)}, f32[64]{0:T(128)}, u32[]{:S(2)}) copy-start(f32[64]{0:T(128)} %param.39) | copy-start | bytes 772
  120.1 25.1 %all-to-all-start.2 = ((bf16[16,7,128]{2,1,0:T(8,128)(2,1)}), bf16[16,7,128]{2,1,0:T(8,128)(2,1)S(1)}, u32[]{:S(2)}, u32[]{:S(2)}) async-start(bf16[16,7,128]{2,1,0:T(8,128)(2,1)} %all_to_all.50), calls=%async_computation.2 | async-start | bytes 65536 | tf_op jit(solution)/shard_map/all_to_all | solution.py:110
  146.4 16.6 %all-to-all-start.3 = ((bf16[16,3,2048]{2,1,0:T(4,128)(2,1)}), bf16[16,3,2048]{2,1,0:T(4,128)(2,1)S(1)}, u32[]{:S(2)}, u32[]{:S(2)}) async-start(bf16[16,3,2048]{2,1,0:T(4,128)(2,1)} %reshape.112), calls=%async_computation.3 | async-start | bytes 524288 | tf_op jit(solution)/shard_map/all_to_all | solution.py:130
  162.9 11.6 %copy-start.4 = (bf16[7,3,4608]{2,0,1:T(8,128)(2,1)S(1)}, bf16[7,3,4608]{2,0,1:T(8,128)(2,1)}, u32[]{:S(2)}) copy-start(bf16[7,3,4608]{2,0,1:T(8,128)(2,1)} %param.25) | copy-start | bytes 580612
  168.5 16.0 %all-to-all-start.4 = ((bf16[16,3,2048]{2,1,0:T(4,128)(2,1)}), bf16[16,3,2048]{2,1,0:T(4,128)(2,1)S(1)}, u32[]{:S(2)}, u32[]{:S(2)}) async-start(bf16[16,3,2048]{2,1,0:T(4,128)(2,1)} %reshape.114), calls=%async_computation.4 | async-start | bytes 524288 | tf_op jit(solution)/shard_map/all_to_all | solution.py:139
where the time goes:
time: 188 us; the launch traced here: 186 us
  blocking collectives  45.3 us (24%)
  matrix products  41.2 us (22%)
  local copies, waits for them, and re-layouts  32.7 us (17%)
  other arithmetic  25.3 us (13%)
  starting transfers between devices  25 us (13%)
  waiting for transfers between devices  15.7 us (8%)
    dot_general x1, matrix products, state_step(): jnp.einsum('bhpn,bhn->bhp', carried, c_heads, precision=lax.Precision.HIG...  26.7 us
    all_gather x1, blocking collectives, body(): row_part = lax.all_gather(normed, 'ep', axis=0, tiled=True)  24.6 us
    all_gather x1, blocking collectives, body(): lax.all_gather(y_mix, 'ep', axis=0, tiled=True)  20.7 us
    mul x1, local copies, waits for them, and re-layouts, state_step(): (step_size[:, :, None] * x_heads)[:, :, :, None] * b_heads[:, :, None, :]  12.9 us
    reshape x1, local copies, waits for them, and re-layouts, state_step(): carried = state_in.reshape(row_count, HEADS, HEAD_DIM, STATE)  12.7 us
    add x1, other arithmetic, state_step(): decay_rate[:, :, None, None] * carried  10.6 us
    all_to_all x1, waiting for transfers between devices, body(): lax.all_to_all(expert_out.reshape(sources, slots_here, width), 'ep', spli...  9.27 us
    mul x1, other arithmetic, state_step(): (step_size[:, :, None] * x_heads)[:, :, :, None] * b_heads[:, :, None, :]  8.67 us
  transfers between devices with their start and end apart: 5, of which 2 were waited for; matrix products, arithmetic and copies ran while one was open for 29% of the time, Pallas kernels for 0%

commit v1 on v0

--- a/solution.py
+++ b/solution.py
@@ -84,10 +84,17 @@
     )
     projected_both = both_parts.astype(jnp.bfloat16)
     col_count = z_weight.shape[1]
+    map_leaves = lambda message, named_axis: jnp.concatenate(
+        lax.all_to_all(
+            jnp.stack(jnp.split(message, lax.axis_size(named_axis), axis=0), axis=0),
+            axis_name=named_axis,
+            split_axis=0,
+            concat_axis=0,
+        ),
+        axis=1,
+    )
     gate_z, x_part = (
-        lax.all_to_all(
-            projected_both[:, :col_count], "ep", split_axis=0, concat_axis=1, tiled=True
-        ),
+        map_leaves(projected_both[:, :col_count], "ep"),
         lax.all_to_all(
             projected_both[:, col_count:], "ep", split_axis=0, concat_axis=1, tiled=True
         ),

time: 188 us -> 195 us (1.037)
  local copies, waits for them, and re-layouts: 32.7 us -> 41 us
    unnamed x29 -> x50, local copies, waits for them, and re-layouts: 1.58 us -> 10.5 us
  transfers between devices with their start and end apart: 5 -> 5, of which waited for: 2 -> 2; matrix products, arithmetic and copies ran while one was open for 29% -> 32% of each run, Pallas kernels for 0% -> 0%
where the time goes in v1:
time: 195 us; the launch traced here: 193 us
  blocking collectives  45.3 us (23%)
  matrix products  41.2 us (21%)
  local copies, waits for them, and re-layouts  41 us (21%)
  starting transfers between devices  25 us (13%)
  other arithmetic  23.8 us (12%)
  waiting for transfers between devices  15.9 us (8%)
    dot_general x1, matrix products, state_step(): jnp.einsum('bhpn,bhn->bhp', carried, c_heads, precision=lax.Precision.HIG...  26.7 us
    all_gather x1, blocking collectives, body(): row_part = lax.all_gather(normed, 'ep', axis=0, tiled=True)  24.6 us
    all_gather x1, blocking collectives, body(): lax.all_gather(y_mix, 'ep', axis=0, tiled=True)  20.7 us
    mul x1, local copies, waits for them, and re-layouts, state_step(): (step_size[:, :, None] * x_heads)[:, :, :, None] * b_heads[:, :, None, :]  12.9 us
    reshape x1, local copies, waits for them, and re-layouts, state_step(): carried = state_in.reshape(row_count, HEADS, HEAD_DIM, STATE)  12.7 us
    add x1, other arithmetic, state_step(): decay_rate[:, :, None, None] * carried  10.6 us
    unnamed x50, local copies, waits for them, and re-layouts  10.5 us
    all_to_all x1, waiting for transfers between devices, body(): lax.all_to_all(expert_out.reshape(sources, slots_here, width), 'ep', spli...  9.27 us
  transfers between devices with their start and end apart: 5, of which 2 were waited for; matrix products, arithmetic and copies ran while one was open for 32% of the time, Pallas kernels for 0%

profile of v1, /device:TPU:0, one launch (start us, length us, event | category | flops | bytes accessed | tf_op | source)
XLA Modules:
  0.0 193.2 jit_solution(4108040612240752034)
XLA Ops:
  0.7 0.8 convert_element_type.99
  1.5 0.9 fusion.30
  2.4 0.8 fusion.52
  3.2 24.6 %all-gather = bf16[16,7,2048]{2,1,0:T(8,128)(2,1)S(1)} all-gather(bf16[1,7,2048]{2,1,0:T(8,128)(2,1)S(1)} %fusion.52), channel_id=1, replica_groups=mesh['grp'=2,'ep'=16] {'ep'}, dimensions={0}, use_global_device_ids=true | all-gather | bytes 487424 | tf_op jit(solution)/shard_map/all_gather | solution.py:77
  28.0 1.5 convolution_convert_fusion.3
  29.5 0.7 all_to_all.37
  30.2 3.5 %all-to-all-start = ((bf16[16,7,256]{2,1,0:T(8,128)(2,1)}), bf16[16,7,256]{2,1,0:T(8,128)(2,1)S(1)}, u32[]{:S(2)}, u32[]{:S(2)}) async-start(bf16[16,7,256]{2,1,0:T(8,128)(2,1)} %all_to_all.37), calls=%async_computation | async-start | bytes 131072 | tf_op jit(solution)/shard_map/all_to_all | solution.py:98
  33.7 1.5 convolution_convert_fusion.2
  35.2 0.6 constant_dynamic-update-slice_fusion.15
  35.8 0.6 constant_dynamic-update-slice_fusion.14
  36.4 0.6 constant_dynamic-update-slice_fusion.13
  37.0 0.6 constant_dynamic-update-slice_fusion.12
  37.6 0.6 constant_dynamic-update-slice_fusion.11
  38.2 0.6 constant_dynamic-update-slice_fusion.10
  38.8 0.6 constant_dynamic-update-slice_fusion.9
  39.4 0.6 constant_dynamic-update-slice_fusion.8
  40.0 0.6 constant_dynamic-update-slice_fusion.7
  40.6 0.6 constant_dynamic-update-slice_fusion.6
  41.2 0.6 constant_dynamic-update-slice_fusion.5
  41.8 0.6 constant_dynamic-update-slice_fusion.4
  42.4 0.6 constant_dynamic-update-slice_fusion.3
  43.0 0.6 constant_dynamic-update-slice_fusion.2
  43.6 0.6 constant_dynamic-update-slice_fusion.1
  44.2 0.6 constant_dynamic-update-slice_fusion
  44.8 1.5 convolution_convert_fusion.5
  46.3 1.5 convolution_convert_fusion.6
  48.0 12.7 %reshape.105 = f32[7,64,64,64]{3,2,1,0:T(8,128)} reshape(f32[7,64,4096]{2,1,0:T(8,128)} %param.24) | data formatting | bytes 14680064 | tf_op jit(solution)/shard_map/reshape | solution.py:36
  62.1 6.0 %all-to-all-start.1 = ((bf16[16,7,256]{2,1,0:T(8,128)(2,1)}), bf16[16,7,256]{2,1,0:T(8,128)(2,1)S(1)}, u32[]{:S(2)}, u32[]{:S(2)}) async-start(bf16[16,7,256]{2,1,0:T(8,128)(2,1)} %constant_dynamic-update-slice_fusion), calls=%async_computation.1 | async-start | bytes 131072 | tf_op jit(solution)/shard_map/all_to_all | solution.py:88
  68.3 6.7 %all-to-all-done.1 = bf16[16,7,256]{2,1,0:T(8,128)(2,1)S(1)} async-done(((bf16[16,7,256]{2,1,0:T(8,128)(2,1)}), bf16[16,7,256]{2,1,0:T(8,128)(2,1)S(1)}, u32[]{:S(2)}, u32[]{:S(2)}) %all-to-all-start.1) | async-done | bytes 57376 | tf_op jit(solution)/shard_map/all_to_all | solution.py:88
  75.6 26.7 %fusion = f32[7,64,1,64]{3,2,1,0:T(1,128)S(1)} fusion(f32[7,64,64,1]{2,3,1,0:T(1,128)S(1)} %bitcast.132, f32[7,64,64,64]{3,2,1,0:T(8,128)} %reshape.105, f32[7,64]{1,0:T(8,128)S(1)} %get-tuple-element.17, f32[7,64,64]{2,1,0:T(8,128)S(1)} %bitcast.129, f32[7,64,64]{2,1,0:T(8,128)S(1)} %broadcast_multiply_fusion.2), kind=kOutput, calls=%fused_computation | convolution fusion | flops 27525120 | bytes 7800576 | tf_op jit(solution)/shard_map/bhpn,bhn->bhp/dot_general | solution.py:41
  102.7 20.7 %all-gather.1 = bf16[16,7,4096]{2,1,0:T(8,128)(2,1)S(1)} all-gather(bf16[1,7,4096]{2,1,0:T(8,128)(2,1)S(1)} %fusion.37), channel_id=1, replica_groups=mesh['grp'=2,'ep'=16] {'ep'}, dimensions={0}, use_global_device_ids=true | all-gather | bytes 974848 | tf_op jit(solution)/shard_map/all_gather | solution.py:113
  123.4 1.2 reshape.120
  124.6 1.9 convolution_convert_fusion.4
  126.5 0.6 all_to_all.42
  127.2 3.5 %all-to-all-start.2 = ((bf16[16,7,128]{2,1,0:T(8,128)(2,1)}), bf16[16,7,128]{2,1,0:T(8,128)(2,1)S(1)}, u32[]{:S(2)}, u32[]{:S(2)}) async-start(bf16[16,7,128]{2,1,0:T(8,128)(2,1)} %all_to_all.42), calls=%async_computation.2 | async-start | bytes 65536 | tf_op jit(solution)/shard_map/all_to_all | solution.py:117
  130.7 8.7 %broadcast_multiply_fusion = f32[7,64,64,64]{3,2,1,0:T(8,128)} fusion(f32[7,64,64]{2,1,0:T(8,128)} %bitcast.130, f32[7,64,64]{2,1,0:T(8,128)S(1)} %broadcast_multiply_fusion.2), kind=kLoop, calls=%fused_computation.4 | loop fusion | flops 1835008 | bytes 7569408 | tf_op jit(solution)/shard_map/mul | solution.py:39
  139.4 12.9 %mul.261 = f32[7,64,4096]{2,1,0:T(8,128)} reshape(f32[7,64,64,64]{3,2,1,0:T(8,128)} %broadcast_multiply_fusion) | data formatting | bytes 14680064 | tf_op jit(solution)/shard_map/mul | solution.py:39
  152.4 0.3 convolution_convert_fusion.1
  152.7 0.8 reshape.111
  153.5 6.0 %all-to-all-start.3 = ((bf16[16,3,2048]{2,1,0:T(4,128)(2,1)}), bf16[16,3,2048]{2,1,0:T(4,128)(2,1)S(1)}, u32[]{:S(2)}, u32[]{:S(2)}) async-start(bf16[16,3,2048]{2,1,0:T(4,128)(2,1)} %reshape.111), calls=%async_computation.3 | async-start | bytes 524288 | tf_op jit(solution)/shard_map/all_to_all | solution.py:137
  159.5 10.6 %multiply_add_fusion = f32[7,64,4096]{2,1,0:T(8,128)} fusion(f32[7,64,4096]{2,1,0:T(8,128)} %mul.261, f32[7,64,4096]{2,1,0:T(8,128)} %param.24, f32[7,64]{1,0:T(8,128)S(1)} %get-tuple-element.17), kind=kLoop, calls=%fused_computation.3 | loop fusion | flops 3670016 | bytes 22021888 | tf_op jit(solution)/shard_map/add | solution.py:38
  170.2 2.0 %fusion.12 = f32[48,512]{1,0:T(8,128)S(1)} fusion(bf16[48,2048]{1,0:T(8,128)(2,1)S(1)} %reshape.112, bf16[1,2048,512]{2,1,0:T(8,128)(2,1)} %param.43), kind=kOutput, calls=%fused_computation.20 | convolution fusion | flops 100663296 | bytes 2392064 | tf_op jit(solution)/shard_map/dot_general | solution.py:140
  172.3 2.5 %convolution_convert_fusion = bf16[48,2048]{1,0:T(8,128)(2,1)S(1)} fusion(bf16[1,512,2048]{2,1,0:T(8,128)(2,1)S(1)} %copy-done, bf16[48,2048]{1,0:T(8,128)(2,1)S(1)} %reshape.112, bf16[1,2048,512]{2,1,0:T(8,128)(2,1)} %param.44, f32[48,512]{1,0:T(8,128)S(1)} %fusion.12), kind=kOutput, calls=%fused_computation.6 | convolution fusion | flops 201572352 | bytes 4685824 | tf_op jit(solution)/shard_map/dot_general | solution.py:143
  174.8 0.8 reshape.113
  175.6 6.0 %all-to-all-start.4 = ((bf16[16,3,2048]{2,1,0:T(4,128)(2,1)}), bf16[16,3,2048]{2,1,0:T(4,128)(2,1)S(1)}, u32[]{:S(2)}, u32[]{:S(2)}) async-start(bf16[16,3,2048]{2,1,0:T(4,128)(2,1)} %reshape.113), calls=%async_computation.4 | async-start | bytes 524288 | tf_op jit(solution)/shard_map/all_to_all | solution.py:146
  181.6 0.7 fusion.24
  182.4 9.3 %all-to-all-done.4 = bf16[16,3,2048]{2,1,0:T(4,128)(2,1)S(1)} async-done(((bf16[16,3,2048]{2,1,0:T(4,128)(2,1)}), bf16[16,3,2048]{2,1,0:T(4,128)(2,1)S(1)}, u32[]{:S(2)}, u32[]{:S(2)}) %all-to-all-start.4) | async-done | bytes 196640 | tf_op jit(solution)/shard_map/all_to_all | solution.py:146
  192.4 0.8 fusion.8
  (80 shorter events, 3.7 us)
Async XLA Ops:
  0.6 171.6 %copy-start = (bf16[1,512,2048]{2,1,0:T(8,128)(2,1)S(1)}, bf16[1,512,2048]{2,1,0:T(8,128)(2,1)}, u32[]{:S(2)}) copy-start(bf16[1,512,2048]{2,1,0:T(8,128)(2,1)} %param.45) | copy-start | bytes 6291460
  0.6 47.2 %copy-start.5 = (bf16[4,4608]{1,0:T(4,128)(2,1)S(1)}, bf16[4,4608]{1,0:T(4,128)(2,1)}, u32[]{:S(2)}) copy-start(bf16[4,4608]{1,0:T(4,128)(2,1)} %param.35) | copy-start | bytes 110596
  0.7 47.2 %copy-start.6 = (bf16[4608]{0:T(1024)(128)(2,1)S(1)}, bf16[4608]{0:T(1024)(128)(2,1)}, u32[]{:S(2)}) copy-start(bf16[4608]{0:T(1024)(128)(2,1)} %param.36) | copy-start | bytes 27652
  0.7 47.2 %copy-start.14 = (f32[64]{0:T(128)S(1)}, f32[64]{0:T(128)}, u32[]{:S(2)}) copy-start(f32[64]{0:T(128)} %param.38) | copy-start | bytes 772
  30.2 31.8 %all-to-all-start = ((bf16[16,7,256]{2,1,0:T(8,128)(2,1)}), bf16[16,7,256]{2,1,0:T(8,128)(2,1)S(1)}, u32[]{:S(2)}, u32[]{:S(2)}) async-start(bf16[16,7,256]{2,1,0:T(8,128)(2,1)} %all_to_all.37), calls=%async_computation | async-start | bytes 131072 | tf_op jit(solution)/shard_map/all_to_all | solution.py:98
  47.9 12.8 %copy-start.7 = (bf16[4096]{0:T(1024)(128)(2,1)S(1)}, bf16[4096]{0:T(1024)(128)(2,1)}, u32[]{:S(2)}) copy-start(bf16[4096]{0:T(1024)(128)(2,1)} %param.40) | copy-start | bytes 24580
  47.9 12.8 %copy-start.10 = (s32[7,4]{0,1:T(4,128)S(1)}, s32[7,4]{0,1:T(4,128)}, u32[]{:S(2)}) copy-start(s32[7,4]{0,1:T(4,128)} %param.26) | copy-start | bytes 340
  47.9 13.5 %copy-start.9 = (bf16[2048]{0:T(1024)(128)(2,1)S(1)}, bf16[2048]{0:T(1024)(128)(2,1)}, u32[]{:S(2)}) copy-start(bf16[2048]{0:T(1024)(128)(2,1)} %param.42) | copy-start | bytes 12292
  48.0 13.5 %copy-start.8 = (f32[7,4]{0,1:T(4,128)S(1)}, f32[7,4]{0,1:T(4,128)}, u32[]{:S(2)}) copy-start(f32[7,4]{0,1:T(4,128)} %param.28) | copy-start | bytes 340
  48.0 13.5 %copy-start.12 = (f32[7]{0:T(128)S(1)}, f32[7]{0:T(128)}, u32[]{:S(2)}) copy-start(f32[7]{0:T(128)} %param.27) | copy-start | bytes 88
  48.0 13.5 %copy-start.2 = (bf16[7,2048]{1,0:T(8,128)(2,1)S(1)}, bf16[7,2048]{1,0:T(8,128)(2,1)}, u32[]{:S(2)}) copy-start(bf16[7,2048]{1,0:T(8,128)(2,1)} %param.23) | copy-start | bytes 86020
  48.0 13.5 %copy-start.13 = (bf16[2048,64]{0,1:T(8,128)(2,1)S(1)}, bf16[2048,64]{0,1:T(8,128)(2,1)}, u32[]{:S(2)}) copy-start(bf16[2048,64]{0,1:T(8,128)(2,1)} %param.34) | copy-start | bytes 786436
  48.0 13.5 %copy-start.15 = (f32[64]{0:T(128)S(1)}, f32[64]{0:T(128)}, u32[]{:S(2)}) copy-start(f32[64]{0:T(128)} %param.37) | copy-start | bytes 772
  48.0 20.0 %copy-start.3 = (bf16[7,3,4608]{2,0,1:T(8,128)(2,1)S(1)}, bf16[7,3,4608]{2,0,1:T(8,128)(2,1)}, u32[]{:S(2)}) copy-start(bf16[7,3,4608]{2,0,1:T(8,128)(2,1)} %param.25) | copy-start | bytes 580612
  62.1 12.9 %all-to-all-start.1 = ((bf16[16,7,256]{2,1,0:T(8,128)(2,1)}), bf16[16,7,256]{2,1,0:T(8,128)(2,1)S(1)}, u32[]{:S(2)}, u32[]{:S(2)}) async-start(bf16[16,7,256]{2,1,0:T(8,128)(2,1)} %constant_dynamic-update-slice_fusion), calls=%async_computation.1 | async-start | bytes 131072 | tf_op jit(solution)/shard_map/all_to_all | solution.py:88
  75.5 26.7 %copy-start.1 = (f32[7,4,16,64]{3,2,1,0:T(8,128)}, f32[7,4,16,64]{3,2,1,0:T(8,128)S(1)}, u32[]{:S(2)}) copy-start(f32[7,4,16,64]{3,2,1,0:T(8,128)S(1)} %broadcast_in_dim.7) | copy-start | bytes 344068
  75.5 26.7 %copy-start.11 = (f32[64]{0:T(128)S(1)}, f32[64]{0:T(128)}, u32[]{:S(2)}) copy-start(f32[64]{0:T(128)} %param.39) | copy-start | bytes 772
  127.2 25.1 %all-to-all-start.2 = ((bf16[16,7,128]{2,1,0:T(8,128)(2,1)}), bf16[16,7,128]{2,1,0:T(8,128)(2,1)S(1)}, u32[]{:S(2)}, u32[]{:S(2)}) async-start(bf16[16,7,128]{2,1,0:T(8,128)(2,1)} %all_to_all.42), calls=%async_computation.2 | async-start | bytes 65536 | tf_op jit(solution)/shard_map/all_to_all | solution.py:117
  153.5 16.6 %all-to-all-start.3 = ((bf16[16,3,2048]{2,1,0:T(4,128)(2,1)}), bf16[16,3,2048]{2,1,0:T(4,128)(2,1)S(1)}, u32[]{:S(2)}, u32[]{:S(2)}) async-start(bf16[16,3,2048]{2,1,0:T(4,128)(2,1)} %reshape.111), calls=%async_computation.3 | async-start | bytes 524288 | tf_op jit(solution)/shard_map/all_to_all | solution.py:137
  170.0 11.6 %copy-start.4 = (bf16[7,3,4608]{2,0,1:T(8,128)(2,1)S(1)}, bf16[7,3,4608]{2,0,1:T(8,128)(2,1)}, u32[]{:S(2)}) copy-start(bf16[7,3,4608]{2,0,1:T(8,128)(2,1)} %param.25) | copy-start | bytes 580612
  175.6 16.0 %all-to-all-start.4 = ((bf16[16,3,2048]{2,1,0:T(4,128)(2,1)}), bf16[16,3,2048]{2,1,0:T(4,128)(2,1)S(1)}, u32[]{:S(2)}, u32[]{:S(2)}) async-start(bf16[16,3,2048]{2,1,0:T(4,128)(2,1)} %reshape.113), calls=%async_computation.4 | async-start | bytes 524288 | tf_op jit(solution)/shard_map/all_to_all | solution.py:146
